TPU v7x, 32 devices: a whole 2x2x4 slice. The times are simulated.
32 devices in a mesh: ep: 8 (over z, core), tp: 4 (over y, x).
Axes of the slice: x: 2, y: 2, z: 4, core: 2. Of those that a mesh axis runs over, the one named last changes fastest.
Arguments:
- queries: bfloat16 [4096, 1024], P('ep', 'tp'), may hold values from -9 to 9
- keys: bfloat16 [4096, 128], P('ep'), may hold values from -6 to 6
- values: bfloat16 [4096, 128], P('ep'), may hold values from -6 to 6
- sink_logits: float32 [16], P('tp'), may hold values from 2 to 7
- out_weight: bfloat16 [1024, 2048], P(None, 'tp'), may hold values from -0.8984375 to 0.8984375
- expert_input: bfloat16 [2048, 2048], P('ep'), may hold values from -6 to 6
- norm_gain: float32 [2048], replicated, may hold values from 0.1 to 1.9
- routes: int32 [2048, 2], P('ep'), may hold values from 0 to 7, all different within a row; in each aligned block of 256 rows (0 to 255, 256 to 511, ...) at most 128 rows name the same one
- route_weights: float32 [2048, 2], P('ep'), may hold values from 0.1 to 1
- gate_weight: bfloat16 [8, 2048, 4096], P('ep', None, 'tp'), may hold values from -0.125 to 0.125
- up_weight: bfloat16 [8, 2048, 4096], P('ep', None, 'tp'), may hold values from -0.125 to 0.125
- down_weight: bfloat16 [8, 4096, 2048], P('ep', 'tp'), may hold values from -0.09375 to 0.09375
Outputs:
- attn_out: bfloat16 [4096, 2048], P('ep', 'tp')
- expert_out: bfloat16 [2048, 2048], P('ep', 'tp')
Inputs may be any that keep to these rules, and one draw needn't show every extreme that they name: `routes`: each row names 2 different experts. Within the rows of one index of ep (aligned blocks of 256 rows) no expert is named by more than 128 rows, and in some blocks one expert is named by exactly 128 rows.
All inputs are finite; a program needn't handle non-finite values.
Results may differ from a plain program's by a relative error of at most 0.015.
Values may be sent and summed in bfloat16 or wider, within the bound.
A program may use at most 64 MiB of HBM per device.

v0:
```python
import jax
import jax.numpy as jnp
from jax import lax
from jax.sharding import PartitionSpec as P

HEADS = 16
KV = 2
HD = 64
WINDOW = 128
rms_eps = 1e-06
mask_value = -1e30


def passed_along(value, axis, steps):
    count = lax.axis_size(axis)
    first, last = (max(0, -steps), min(count, count - steps))
    return lax.ppermute(value, axis, [(source, source + steps) for source in range(first, last)])


def rotate_heads(values_in, positions):
    half_dim = values_in.shape[-1] // 2
    inv_freq = 10000.0 ** (-jnp.arange(half_dim, dtype=jnp.float32) * (2.0 / values_in.shape[-1]))
    angles = positions[:, None] * inv_freq[None, :]
    cosine_table = jnp.cos(angles)[:, None, :]
    sine_table = jnp.sin(angles)[:, None, :]
    first_half = values_in[..., :half_dim]
    second_half = values_in[..., half_dim:]
    return jnp.concatenate(
        [
            first_half * cosine_table - second_half * sine_table,
            second_half * cosine_table + first_half * sine_table,
        ],
        axis=-1,
    )


def local(
    queries,
    keys,
    values,
    sink_logits,
    out_weight,
    expert_input,
    norm_gain,
    routes,
    route_weights,
    gate_weight,
    up_weight,
    down_weight,
):
    seq_rows = queries.shape[0]
    heads_here = queries.shape[1] // HD
    group_size = HEADS // KV
    kv_here = max(1, heads_here // group_size)
    heads_per_kv = heads_here // kv_here
    kv_first = lax.axis_index("tp") * heads_here // group_size
    key_local = lax.dynamic_slice_in_dim(keys, kv_first * HD, kv_here * HD, 1)
    value_local = lax.dynamic_slice_in_dim(values, kv_first * HD, kv_here * HD, 1)
    offset = lax.axis_index("ep") * seq_rows
    positions = (offset + jnp.arange(seq_rows, dtype=jnp.int32)).astype(jnp.float32)
    query_rot = rotate_heads(
        queries.astype(jnp.float32).reshape(seq_rows, heads_here, HD), positions
    ).astype(jnp.bfloat16)
    key_rot = rotate_heads(
        key_local.astype(jnp.float32).reshape(seq_rows, kv_here, HD), positions
    ).astype(jnp.bfloat16)
    value_heads = value_local.reshape(seq_rows, kv_here, HD)
    rim_pair = jnp.concatenate(
        [
            key_rot.reshape(seq_rows, kv_here * HD)[seq_rows - WINDOW :],
            value_local[seq_rows - WINDOW :],
        ],
        axis=1,
    )
    rim_pair = passed_along(rim_pair, "ep", 1)
    rim_key = rim_pair[:, : kv_here * HD].reshape(WINDOW, kv_here, HD)
    rim_value = rim_pair[:, kv_here * HD :].reshape(WINDOW, kv_here, HD)
    blocks = seq_rows // WINDOW

    def band_of(rim_part, local_part):
        padded = jnp.concatenate([rim_part, local_part], axis=0)
        earlier = padded[:seq_rows].reshape(blocks, WINDOW, kv_here, HD)
        current = padded[WINDOW:].reshape(blocks, WINDOW, kv_here, HD)
        return jnp.concatenate([earlier, current], axis=1)

    key_band = band_of(rim_key, key_rot)
    value_band = band_of(rim_value, value_heads)
    query_blocks = query_rot.reshape(blocks, WINDOW, kv_here, heads_per_kv, HD)
    scores = jnp.einsum(
        "nqhgd,nkhd->nhgqk", query_blocks, key_band, preferred_element_type=jnp.float32
    ) * HD ** (-0.5)
    block_start = offset + jnp.arange(blocks, dtype=jnp.int32)[:, None, None] * WINDOW
    query_pos = block_start + jnp.arange(WINDOW, dtype=jnp.int32)[None, :, None]
    key_pos = block_start - WINDOW + jnp.arange(2 * WINDOW, dtype=jnp.int32)[None, None, :]
    distance = query_pos - key_pos
    allowed = (distance >= 0) & (distance < WINDOW) & (key_pos >= 0)
    scores = jnp.where(allowed[:, None, None], scores, mask_value)
    sink_row = sink_logits.reshape(1, kv_here, heads_per_kv, 1)
    row_top = jnp.maximum(jnp.max(scores, axis=-1), sink_row)
    exp_scores = jnp.exp(scores - row_top[..., None])
    row_total = jnp.sum(exp_scores, axis=-1) + jnp.exp(sink_row - row_top)
    weights = (exp_scores / row_total[..., None]).astype(jnp.bfloat16)
    head_mix = jnp.einsum(
        "nhgqk,nkhd->nqhgd", weights, value_band, preferred_element_type=jnp.float32
    )
    head_mix = head_mix.astype(jnp.bfloat16).reshape(seq_rows, heads_here * HD)
    attn_out = jnp.dot(
        lax.all_gather(head_mix, "tp", axis=1, tiled=True),
        out_weight,
        preferred_element_type=jnp.float32,
    ).astype(jnp.bfloat16)
    token_rows = expert_input.shape[0]
    top_count = routes.shape[1]
    expert_count = lax.axis_size("ep")
    capacity = 2 * top_count * token_rows // expert_count
    slot_total = expert_count * capacity
    input_wide = expert_input.astype(jnp.float32)
    inv_rms = lax.rsqrt(jnp.mean(input_wide * input_wide, axis=-1, keepdims=True) + rms_eps)
    normed = (input_wide * inv_rms * norm_gain[None, :]).astype(jnp.bfloat16)
    flat_expert = routes.reshape(-1)
    one_hot = (flat_expert[:, None] == jnp.arange(expert_count, dtype=jnp.int32)[None, :]).astype(
        jnp.int32
    )
    route_rank = jnp.sum(jnp.cumsum(one_hot, axis=0) * one_hot, axis=1) - 1
    slot_of_route = flat_expert * capacity + route_rank
    matches = slot_of_route[None, :] == jnp.arange(slot_total, dtype=jnp.int32)[:, None]
    route_token = jnp.arange(token_rows * top_count, dtype=jnp.int32) // top_count
    source_row = jnp.sum(jnp.where(matches, route_token[None, :] + 1, 0), axis=1) - 1
    occupied = source_row >= 0
    gate_local = gate_weight[0]
    up_local = up_weight[0]
    down_local = down_weight[0]
    column_count = normed.shape[1] // lax.axis_size("tp")
    own_columns = lax.dynamic_slice_in_dim(
        normed, lax.axis_index("tp") * column_count, column_count, 1
    )
    slot_rows = jnp.where(
        occupied[:, None],
        jnp.take(own_columns, jnp.maximum(source_row, 0), axis=0),
        jnp.zeros((), jnp.bfloat16),
    )
    outgoing = slot_rows.reshape(expert_count, capacity, column_count)
    arrived = lax.all_to_all(outgoing, "ep", split_axis=0, concat_axis=0, tiled=True)
    leading = arrived.shape[:2]
    portion = lax.all_gather(arrived, "tp", axis=2, tiled=True)
    flat_piece = portion.reshape(-1, portion.shape[2])
    gate_acc = jnp.dot(flat_piece, gate_local, preferred_element_type=jnp.float32)
    up_acc = jnp.dot(flat_piece, up_local, preferred_element_type=jnp.float32)
    hidden = (jax.nn.silu(gate_acc) * up_acc).astype(jnp.bfloat16)
    summed = lax.psum_scatter(
        lax.dot_general(
            down_local, hidden, (((0,), (1,)), ((), ())), preferred_element_type=jnp.float32
        ).astype(jnp.bfloat16),
        "tp",
        scatter_dimension=0,
        tiled=True,
    ).astype(jnp.float32)
    returned = summed.astype(jnp.bfloat16).reshape((summed.shape[0],) + leading)
    results_home = lax.all_to_all(returned, "ep", split_axis=1, concat_axis=1, tiled=True)
    home_flat = results_home.reshape(results_home.shape[0], -1)
    picked = jnp.take(home_flat, slot_of_route, axis=1).astype(jnp.float32)
    weighted = picked * route_weights.reshape(1, -1)
    combined = jnp.sum(weighted.reshape(results_home.shape[0], token_rows, top_count), axis=2)
    expert_out = combined.T.astype(jnp.bfloat16)
    return (attn_out, expert_out)


def solution(mesh):
    return jax.shard_map(
        local,
        mesh=mesh,
        in_specs=(
            P("ep", "tp"),
            P("ep", None),
            P("ep", None),
            P("tp"),
            P(None, "tp"),
            P("ep", None),
            P(),
            P("ep", None),
            P("ep", None),
            P("ep", None, "tp"),
            P("ep", None, "tp"),
            P("ep", "tp", None),
        ),
        out_specs=(P("ep", "tp"), P("ep", "tp")),
        check_vma=False,
    )
```

profile of v0, /device:TPU:0, one launch (start us, length us, event | category | flops | bytes accessed | tf_op | source)
XLA Modules:
  0.0 217.6 jit_solution(8200057702894979410)
XLA Ops:
  7.2 0.0 copy-start
  7.2 0.0 all-gather.5.cloned.1.call-start
  7.2 1.5 convert_element_type.82
  8.8 1.5 multiply_reduce_fusion
  10.3 0.1 copy.80
  10.4 0.1 eq.39
  10.6 0.1 reshape.508
  10.7 1.1 reduce-window.6
  11.9 0.2 slice_reduce_fusion
  12.1 0.1 fusion.39
  12.2 0.3 select_reduce_fusion
  12.6 0.8 dynamic-slice
  13.4 0.1 fusion.14
  13.5 4.0 %gather_fusion = bf16[1024,512]{1,0:T(8,128)(2,1)S(1)} fusion(bf16[256,512]{1,0:T(8,128)(2,1)S(1)} %fusion.14, s32[1024]{0:T(1024)S(1)} %maximum_clamp_fusion), kind=kCustom, calls=%fused_computation | custom fusion | bytes 2101248 | tf_op jit(solution)/shard_map/jit(_take)/gather | solution.py:139
  17.5 0.5 select_select_fusion
  17.9 32.8 %all_to_all.10 = bf16[8,128,512]{2,1,0:T(8,128)(2,1)} all-to-all(bf16[8,128,512]{2,1,0:T(8,128)(2,1)S(1)} %select_select_fusion), channel_id=1, replica_groups=mesh['ep'=8,'tp'=4] {'ep'}, dimensions={0} | all-to-all | bytes 2097152 | tf_op jit(solution)/shard_map/all_to_all | solution.py:143
  50.7 0.0 all-gather.5.cloned.1.call-update
  50.8 0.0 reduce-scatter.2.cloned.1.call-start
  50.8 51.5 %all-gather.5.cloned.1.call-done = bf16[8,128,2048]{2,1,0:T(8,128)(2,1)} async-done(((bf16[8,128,512]{2,1,0:T(8,128)(2,1)}), bf16[8,128,2048]{2,1,0:T(8,128)(2,1)}) %all-gather.5.cloned.1.call-update) | async-done | bytes 4194320 | tf_op jit(solution)/shard_map/all_gather | solution.py:145
  102.3 7.6 %fusion.2 = f32[1024,1024]{1,0:T(8,128)S(1)} fusion(bf16[1024,2048]{1,0:T(8,128)(2,1)} %bitcast.127, bf16[1,2048,1024]{2,1,0:T(8,128)(2,1)} %param.22), kind=kOutput, calls=%fused_computation.4 | convolution fusion | flops 4294967296 | bytes 12582912 | tf_op jit(solution)/shard_map/dot_general | solution.py:148
  110.0 0.0 copy-start.8
  110.0 5.4 %multiply_convert_fusion = bf16[1024,1024]{1,0:T(8,128)(2,1)S(1)} fusion(f32[1024,1024]{1,0:T(8,128)S(1)} %fusion.2, bf16[1024,2048]{1,0:T(8,128)(2,1)S(1)} %bitcast.128, bf16[1,2048,1024]{2,1,0:T(8,128)(2,1)S(1)} %copy-done.7), kind=kOutput, calls=%fused_computation.9 | convolution fusion | flops 4301258752 | bytes 14680064 | tf_op jit(solution)/shard_map/dot_general | solution.py:147
  115.4 6.1 %convert_bitcast_fusion = bf16[2048,1024]{0,1:T(8,128)(2,1)} fusion(bf16[1024,1024]{1,0:T(8,128)(2,1)S(1)} %multiply_convert_fusion, bf16[1,1024,2048]{2,1,0:T(8,128)(2,1)S(1)} %copy-done.8), kind=kOutput, calls=%fused_computation.8 | convolution fusion | flops 4297064448 | bytes 10485760 | tf_op jit(solution)/shard_map/dot_general | solution.py:151
  121.4 0.0 reduce-scatter.2.cloned.1.call-update
  121.5 0.0 copy-start.6
  121.5 0.0 all-gather.3.cloned.1.call-start
  121.5 0.8 copy-done.2
  122.3 0.1 copy-done.3
  122.4 0.1 constant_dynamic-slice_fusion
  122.5 0.1 copy.89
  122.7 0.1 copy.90
  122.8 0.3 fusion.33
  123.2 1.6 collective-permute-start
  124.8 0.1 copy.75
  124.9 0.1 convert.25
  125.0 0.1 broadcast_compare_fusion
  125.1 0.1 iota_add_fusion.1
  125.1 0.1 iota_add_fusion
  125.2 0.3 multiply_cosine_fusion
  125.5 0.3 fusion.16
  125.9 0.1 fusion.20
  126.1 0.0 collective-permute-done
  126.1 0.5 fusion.47
  126.6 0.1 broadcast_maximum_fusion
  126.7 0.3 fusion.10
  127.0 0.1 exponential_add_fusion
  127.1 0.5 fusion.11
  127.6 0.2 copy.79
  127.8 0.7 copy.105
  128.6 0.0 all-gather.3.cloned.1.call-update
  128.6 45.6 %reduce-scatter.2.cloned.1.call-done = bf16[512,1024]{0,1:T(8,128)(2,1)} async-done(((bf16[2048,1024]{0,1:T(8,128)(2,1)}), bf16[512,1024]{0,1:T(8,128)(2,1)}) %reduce-scatter.2.cloned.1.call-update) | async-done | bytes 1048592 | tf_op jit(solution)/shard_map/reduce_scatter | solution.py:150
  174.2 4.6 %all-to-all-start.1 = ((bf16[512,8,128]{0,2,1:T(8,128)(2,1)}), bf16[512,8,128]{0,2,1:T(8,128)(2,1)S(1)}, u32[]{:S(2)}, u32[]{:S(2)}) async-start(bf16[512,8,128]{0,2,1:T(8,128)(2,1)} %bitcast.120), calls=%async_computation.2 | async-start | bytes 2097152 | tf_op jit(solution)/shard_map/all_to_all | solution.py:159
  178.8 0.1 copy.84
  179.0 0.1 mul.228
  179.1 0.1 sub.79
  179.3 0.1 copy.82
  179.4 0.2 copy.83
  179.6 0.1 copy.85
  179.7 23.4 %all-gather.3.cloned.1.call-done = bf16[512,1024]{0,1:T(8,128)(2,1)} async-done(((bf16[512,256]{0,1:T(8,128)(2,1)}), bf16[512,1024]{0,1:T(8,128)(2,1)}) %all-gather.3.cloned.1.call-update) | async-done | bytes 1048592 | tf_op jit(solution)/shard_map/all_gather | solution.py:108
  203.2 2.8 %convolution_convert_fusion = bf16[512,512]{1,0:T(8,128)(2,1)} fusion(bf16[512,1024]{0,1:T(8,128)(2,1)} %all-gather.3.cloned.1.call-done, bf16[1024,512]{1,0:T(8,128)(2,1)S(1)} %copy-done), kind=kOutput, calls=%fused_computation.17 | convolution fusion | flops 537133056 | bytes 2621440 | tf_op jit(solution)/shard_map/dot_general | solution.py:107
  205.9 0.0 all-to-all-done.1
  205.9 2.0 gather_fusion.1
  207.9 0.2 gather.15
  208.1 2.9 %multiply_reduce_fusion.1 = bf16[512,256]{0,1:T(8,128)(2,1)} fusion(bf16[512,256,2]{0,2,1:T(2,128)(2,1)S(1)} %gather.15, pred[256,2]{1,0:T(8,128)(4,1)S(1)} %copy.83, f32[256,2]{1,0:T(8,128)S(1)} %copy.85), kind=kLoop, calls=%fused_computation.21 | loop fusion | flops 917504 | bytes 788992 | tf_op jit(solution)/shard_map/reduce_sum | solution.py:163
  (41 shorter events, 0.3 us)
Async XLA Ops:
  7.2 196.0 %copy-start = (bf16[1024,512]{1,0:T(8,128)(2,1)S(1)}, bf16[1024,512]{1,0:T(8,128)(2,1)}, u32[]{:S(2)}) copy-start(bf16[1024,512]{1,0:T(8,128)(2,1)} %param.16) | copy-start | bytes 3145732
  7.2 3.1 %copy-start.4 = (s32[256,2]{0,1:T(2,128)S(1)}, s32[256,2]{0,1:T(2,128)}, u32[]{:S(2)}) copy-start(s32[256,2]{0,1:T(2,128)} %param.19) | copy-start | bytes 6148
  7.2 95.1 %all-gather.5.cloned.1.call-start = ((), (), s32[]{:S(2)}) async-start(), calls=%async_computation.4 | async-start | bytes 5242880 | tf_op jit(solution)/shard_map/all_gather | solution.py:145
  50.8 123.5 %reduce-scatter.2.cloned.1.call-start = ((), (), s32[]{:S(2)}) async-start(), calls=%async_computation.5 | async-start | bytes 5242880 | tf_op jit(solution)/shard_map/reduce_scatter | solution.py:150
  102.3 7.7 %copy-start.7 = (bf16[1,2048,1024]{2,1,0:T(8,128)(2,1)S(1)}, bf16[1,2048,1024]{2,1,0:T(8,128)(2,1)}, u32[]{:S(2)}) copy-start(bf16[1,2048,1024]{2,1,0:T(8,128)(2,1)} %param.21) | copy-start | bytes 12582916
  102.3 7.7 %copy-start.9 = (bf16[8,128,2048]{2,1,0:T(8,128)(2,1)S(1)}, bf16[8,128,2048]{2,1,0:T(8,128)(2,1)}, u32[]{:S(2)}) copy-start(bf16[8,128,2048]{2,1,0:T(8,128)(2,1)} %all-gather.5.cloned.1.call-done) | copy-start | bytes 12582916
  110.0 5.4 %copy-start.8 = (bf16[1,1024,2048]{2,1,0:T(8,128)(2,1)S(1)}, bf16[1,1024,2048]{2,1,0:T(8,128)(2,1)}, u32[]{:S(2)}) copy-start(bf16[1,1024,2048]{2,1,0:T(8,128)(2,1)} %param.23) | copy-start | bytes 12582916
  121.4 0.9 copy-start.2
  121.4 1.0 copy-start.3
  121.4 3.3 %copy-start.1 = (bf16[512,256]{1,0:T(8,128)(2,1)S(1)}, bf16[512,256]{1,0:T(8,128)(2,1)}, u32[]{:S(2)}) copy-start(bf16[512,256]{1,0:T(8,128)(2,1)} %param.12) | copy-start | bytes 786436
  121.5 5.2 %copy-start.6 = (f32[4]{0:T(128)S(1)}, f32[4]{0:T(128)}, u32[]{:S(2)}) copy-start(f32[4]{0:T(128)} %param.15) | copy-start | bytes 52
  121.5 81.7 %all-gather.3.cloned.1.call-start = ((), (), s32[]{:S(2)}) async-start(), calls=%async_computation.3 | async-start | bytes 1310720 | tf_op jit(solution)/shard_map/all_gather | solution.py:108
  123.2 2.9 %collective-permute-start = (bf16[128,128]{0,1:T(8,128)(2,1)S(1)}, bf16[128,128]{0,1:T(8,128)(2,1)S(1)}, u32[]{:S(2)}, u32[]{:S(2)}) collective-permute-start(bf16[128,128]{0,1:T(8,128)(2,1)S(1)} %pad_maximum_fusion.3), channel_id=1, source_target_pairs={{0,4},{4,8},{8,12},{12,16},{16,20},{20,24},{24,28},{1,5},{5,9},{9,... | collective-permute-start | bytes 98312 | tf_op jit(solution)/shard_map/ppermute | solution.py:17
  127.1 52.5 %copy-start.5 = (f32[256,2]{0,1:T(2,128)S(1)}, f32[256,2]{0,1:T(2,128)}, u32[]{:S(2)}) copy-start(f32[256,2]{0,1:T(2,128)} %param.20) | copy-start | bytes 6148
  174.2 31.7 %all-to-all-start.1 = ((bf16[512,8,128]{0,2,1:T(8,128)(2,1)}), bf16[512,8,128]{0,2,1:T(8,128)(2,1)S(1)}, u32[]{:S(2)}, u32[]{:S(2)}) async-start(bf16[512,8,128]{0,2,1:T(8,128)(2,1)} %bitcast.120), calls=%async_computation.2 | async-start | bytes 2097152 | tf_op jit(solution)/shard_map/all_to_all | solution.py:159
Sparse Core Ops, SparseCore 0:
  50.9 51.3 all-gather.4
  121.6 52.5 reduce-scatter.1
  176.6 26.4 all-gather.2
where the time goes:
time: 218 us
  waiting for transfers between devices  121 us (56%)
  blocking collectives  32.8 us (15%)
  matrix products  22.8 us (10%)
  between operations  14.2 us (7%)
  local copies, waits for them, and re-layouts  10.8 us (5%)
  other arithmetic  10 us (5%)
  starting transfers between devices  6.3 us (3%)
    all_gather x1, waiting for transfers between devices, local(): portion = lax.all_gather(arrived, 'tp', axis=2, tiled=True)  51.5 us
    reduce_scatter x1, waiting for transfers between devices, local(): lax.psum_scatter(lax.dot_general(down_local, hidden, (((0,), (1,)), ((),...  45.6 us
    all_to_all x1, blocking collectives, local(): lax.all_to_all(outgoing, 'ep', split_axis=0, concat_axis=0, tiled=True)  32.8 us
    all_gather x1, waiting for transfers between devices, local(): lax.all_gather(head_mix, 'tp', axis=1, tiled=True)  23.4 us
    dot_general x1, matrix products, local(): up_acc = jnp.dot(flat_piece, up_local, preferred_element_type=jnp.float32)  7.64 us
    dot_general x1, matrix products, local(): lax.dot_general(down_local, hidden, (((0,), (1,)), ((), ())), preferred_e...  6.07 us
    dot_general x1, matrix products, local(): jnp.dot(flat_piece, gate_local, preferred_element_type=jnp.float32)  5.35 us
    all_to_all x1, starting transfers between devices, local(): lax.all_to_all(returned, 'ep', split_axis=1, concat_axis=1, tiled=True)  4.61 us
  transfers between devices with their start and end apart: 5, of which 3 were waited for; matrix products, arithmetic and copies ran while one was open for 4% of the time, Pallas kernels for 0%

commit v1 on v0

--- a/solution.py
+++ b/solution.py
@@ -142,7 +142,10 @@
     outgoing = slot_rows.reshape(expert_count, capacity, column_count)
     arrived = lax.all_to_all(outgoing, "ep", split_axis=0, concat_axis=0, tiled=True)
     leading = arrived.shape[:2]
-    portion = lax.all_gather(arrived, "tp", axis=2, tiled=True)
+    size = lax.axis_size("tp")
+    pieces = jnp.stack([arrived for _ in range(size)])
+    pieces = lax.all_to_all(pieces, "tp", split_axis=0, concat_axis=0)
+    portion = jnp.concatenate(pieces, axis=2)
     flat_piece = portion.reshape(-1, portion.shape[2])
     gate_acc = jnp.dot(flat_piece, gate_local, preferred_element_type=jnp.float32)
     up_acc = jnp.dot(flat_piece, up_local, preferred_element_type=jnp.float32)

time: 218 us -> 225 us (1.032)
  waiting for transfers between devices: 121 us -> 67.3 us
  blocking collectives: 32.8 us -> 84 us
  matrix products: 22.8 us -> 26.1 us
  local copies, waits for them, and re-layouts: 10.8 us -> 14 us
  other arithmetic: 10 us -> 12.4 us
    all_gather x1 -> x0, waiting for transfers between devices: 51.5 us -> none  [local(): portion = lax.all_gather(arrived, 'tp', axis=2, tiled=True)]
    all_to_all x0 -> x1, blocking collectives: none -> 51.3 us  [local(): pieces = lax.all_to_all(pieces, 'tp', split_axis=0, concat_axis=0)]
    dot_general x1, matrix products: 6.07 us -> 16.3 us  [local(): lax.dot_general(down_local, hidden, (((0,), (1,)), ((), ())), preferred_e...]
    dot_general x1 -> x0, matrix products: 5.35 us -> none  [local(): jnp.dot(flat_piece, gate_local, preferred_element_type=jnp.float32)]
  transfers between devices with their start and end apart: 5 -> 4, of which waited for: 3 -> 2; matrix products, arithmetic and copies ran while one was open for 4% -> 4% of each run, Pallas kernels for 0% -> 0%
where the time goes in v1:
time: 225 us; the launch traced here: 224 us
  blocking collectives  84 us (37%)
  waiting for transfers between devices  67.3 us (30%)
  matrix products  26.1 us (12%)
  between operations  14.5 us (6%)
  local copies, waits for them, and re-layouts  14 us (6%)
  other arithmetic  12.4 us (6%)
  starting transfers between devices  6.16 us (3%)
    all_to_all x1, blocking collectives, local(): pieces = lax.all_to_all(pieces, 'tp', split_axis=0, concat_axis=0)  51.3 us
    reduce_scatter x1, waiting for transfers between devices, local(): lax.psum_scatter(lax.dot_general(down_local, hidden, (((0,), (1,)), ((),...  43.8 us
    all_to_all x1, blocking collectives, local(): lax.all_to_all(outgoing, 'ep', split_axis=0, concat_axis=0, tiled=True)  32.7 us
    all_gather x1, waiting for transfers between devices, local(): lax.all_gather(head_mix, 'tp', axis=1, tiled=True)  23.4 us
    dot_general x1, matrix products, local(): lax.dot_general(down_local, hidden, (((0,), (1,)), ((), ())), preferred_e...  16.3 us
    dot_general x1, matrix products, local(): up_acc = jnp.dot(flat_piece, up_local, preferred_element_type=jnp.float32)  6.09 us
    all_to_all x1, starting transfers between devices, local(): lax.all_to_all(returned, 'ep', split_axis=1, concat_axis=1, tiled=True)  4.61 us
  transfers between devices with their start and end apart: 4, of which 2 were waited for; matrix products, arithmetic and copies ran while one was open for 4% of the time, Pallas kernels for 0%

profile of v1, /device:TPU:0, one launch (start us, length us, event | category | flops | bytes accessed | tf_op | source)
XLA Modules:
  0.0 224.5 jit_solution(3690234468721573864)
XLA Ops:
  7.2 0.0 copy-start
  7.2 0.0 copy-start.5
  7.2 0.0 reduce-scatter.2.cloned.1.call-start
  7.2 2.9 %convert_element_type.82 = f32[256,2048]{1,0:T(8,128)} convert(bf16[256,2048]{1,0:T(8,128)(2,1)} %param.17) | non-fusion elementwise | flops 524288 | bytes 3145728 | tf_op jit(solution)/shard_map/convert_element_type | solution.py:117
  10.1 1.5 multiply_reduce_fusion
  11.7 0.1 copy.83
  11.8 0.1 eq.39
  11.9 0.1 reshape.510
  12.1 1.1 reduce-window.6
  13.2 0.2 slice_reduce_fusion
  13.5 0.1 fusion.50
  13.6 0.3 select_reduce_fusion
  14.0 0.8 dynamic-slice
  14.7 1.1 fusion.25
  15.9 4.0 %gather_fusion = bf16[1024,512]{1,0:T(8,128)(2,1)S(1)} fusion(bf16[256,512]{1,0:T(8,128)(2,1)S(1)} %fusion.25, s32[1024]{0:T(1024)S(1)} %maximum_clamp_fusion), kind=kCustom, calls=%fused_computation | custom fusion | bytes 2101248 | tf_op jit(solution)/shard_map/jit(_take)/gather | solution.py:139
  19.8 0.5 select_select_fusion
  20.3 32.7 %all_to_all.15 = bf16[8,128,512]{2,1,0:T(8,128)(2,1)S(1)} all-to-all(bf16[8,128,512]{2,1,0:T(8,128)(2,1)S(1)} %select_select_fusion), channel_id=1, replica_groups=mesh['ep'=8,'tp'=4] {'ep'}, dimensions={0} | all-to-all | bytes 2097152 | tf_op jit(solution)/shard_map/all_to_all | solution.py:143
  53.0 0.7 copy.87
  53.8 0.5 stack.2
  54.3 0.0 copy-start.8
  54.3 51.3 %all_to_all.16 = bf16[4,8,128,512]{2,1,3,0:T(8,128)(2,1)S(1)} all-to-all(bf16[4,8,128,512]{2,1,3,0:T(8,128)(2,1)S(1)} %stack.2), channel_id=1, replica_groups=mesh['ep'=8,'tp'=4] {'tp'}, dimensions={0} | all-to-all | bytes 8388608 | tf_op jit(solution)/shard_map/all_to_all | solution.py:147
  105.6 2.0 copy-done.1
  107.6 6.1 %fusion = f32[1024,1024]{1,0:T(8,128)} fusion(bf16[1,2048,1024]{2,1,0:T(8,128)(2,1)S(1)} %copy-done.8, bf16[256,8,8,128]{3,2,1,0:T(8,128)(2,1)S(1)} %bitcast.130), kind=kOutput, calls=%fused_computation.2 | convolution fusion | flops 4294967296 | bytes 12582912 | tf_op jit(solution)/shard_map/dot_general | solution.py:151
  113.7 16.3 %convert_bitcast_fusion = bf16[2048,1024]{0,1:T(8,128)(2,1)} fusion(bf16[1,1024,2048]{2,1,0:T(8,128)(2,1)} %param.23, f32[1024,1024]{1,0:T(8,128)} %fusion, bf16[1,2048,1024]{2,1,0:T(8,128)(2,1)} %param.21, bf16[256,8,8,128]{3,2,1,0:T(8,128)(2,1)} %bitcast.131), kind=kOutput, calls=%fused_computation.10 | convolution fusion | flops 8598323200 | bytes 20971520 | tf_op jit(solution)/shard_map/dot_general | solution.py:154
  130.0 0.0 reduce-scatter.2.cloned.1.call-update
  130.0 0.0 copy-start.7
  130.0 0.0 all-gather.2.cloned.1.call-start
  130.1 0.8 copy-done.3
  130.8 0.1 copy-done.4
  130.9 0.1 constant_dynamic-slice_fusion
  131.1 0.1 copy.93
  131.2 0.1 copy.94
  131.3 0.3 fusion.44
  131.7 1.5 collective-permute-start
  133.2 0.1 copy.78
  133.4 0.1 broadcast_compare_fusion
  133.5 0.1 iota_add_fusion.1
  133.5 0.1 iota_add_fusion
  133.6 0.3 multiply_cosine_fusion
  133.9 0.3 fusion.27
  134.3 0.1 fusion.31
  134.5 0.0 collective-permute-done
  134.5 0.5 fusion.59
  135.0 0.1 broadcast_maximum_fusion
  135.1 0.3 fusion.21
  135.4 0.1 exponential_add_fusion
  135.5 0.5 fusion.22
  136.0 0.2 copy.82
  136.2 0.7 copy.122
  137.0 0.0 all-gather.2.cloned.1.call-update
  137.0 43.8 %reduce-scatter.2.cloned.1.call-done = bf16[512,1024]{0,1:T(8,128)(2,1)} async-done(((bf16[2048,1024]{0,1:T(8,128)(2,1)}), bf16[512,1024]{0,1:T(8,128)(2,1)}) %reduce-scatter.2.cloned.1.call-update) | async-done | bytes 1048592 | tf_op jit(solution)/shard_map/reduce_scatter | solution.py:153
  180.8 4.6 %all-to-all-start.2 = ((bf16[512,8,128]{0,2,1:T(8,128)(2,1)}), bf16[512,8,128]{0,2,1:T(8,128)(2,1)S(1)}, u32[]{:S(2)}, u32[]{:S(2)}) async-start(bf16[512,8,128]{0,2,1:T(8,128)(2,1)} %bitcast.134), calls=%async_computation.3 | async-start | bytes 2097152 | tf_op jit(solution)/shard_map/all_to_all | solution.py:162
  185.4 0.1 copy.88
  185.5 0.1 mul.228
  185.7 0.1 sub.79
  185.8 0.1 copy.85
  185.9 0.2 copy.86
  186.1 0.1 copy.89
  186.3 23.4 %all-gather.2.cloned.1.call-done = bf16[512,1024]{0,1:T(8,128)(2,1)} async-done(((bf16[512,256]{0,1:T(8,128)(2,1)}), bf16[512,1024]{0,1:T(8,128)(2,1)}) %all-gather.2.cloned.1.call-update) | async-done | bytes 1048592 | tf_op jit(solution)/shard_map/all_gather | solution.py:108
  209.7 2.7 %convolution_convert_fusion = bf16[512,512]{1,0:T(8,128)(2,1)} fusion(bf16[512,1024]{0,1:T(8,128)(2,1)} %all-gather.2.cloned.1.call-done, bf16[1024,512]{1,0:T(8,128)(2,1)S(1)} %copy-done), kind=kOutput, calls=%fused_computation.22 | convolution fusion | flops 537133056 | bytes 2621440 | tf_op jit(solution)/shard_map/dot_general | solution.py:107
  212.5 0.0 all-to-all-done.2
  212.5 2.0 gather_fusion.1
  214.5 0.2 gather.15
  214.7 2.9 %multiply_reduce_fusion.1 = bf16[512,256]{0,1:T(8,128)(2,1)} fusion(bf16[512,256,2]{0,2,1:T(2,128)(2,1)S(1)} %gather.15, pred[256,2]{1,0:T(8,128)(4,1)S(1)} %copy.86, f32[256,2]{1,0:T(8,128)S(1)} %copy.89), kind=kLoop, calls=%fused_computation.26 | loop fusion | flops 917504 | bytes 788992 | tf_op jit(solution)/shard_map/reduce_sum | solution.py:166
  (38 shorter events, 0.3 us)
Async XLA Ops:
  7.2 202.6 %copy-start = (bf16[1024,512]{1,0:T(8,128)(2,1)S(1)}, bf16[1024,512]{1,0:T(8,128)(2,1)}, u32[]{:S(2)}) copy-start(bf16[1024,512]{1,0:T(8,128)(2,1)} %param.16) | copy-start | bytes 3145732
  7.2 4.5 %copy-start.5 = (s32[256,2]{0,1:T(2,128)S(1)}, s32[256,2]{0,1:T(2,128)}, u32[]{:S(2)}) copy-start(s32[256,2]{0,1:T(2,128)} %param.19) | copy-start | bytes 6148
  7.2 173.6 %reduce-scatter.2.cloned.1.call-start = ((), (), s32[]{:S(2)}) async-start(), calls=%async_computation.5 | async-start | bytes 5242880 | tf_op jit(solution)/shard_map/reduce_scatter | solution.py:153
  54.3 53.2 %copy-start.8 = (bf16[1,2048,1024]{2,1,0:T(8,128)(2,1)S(1)}, bf16[1,2048,1024]{2,1,0:T(8,128)(2,1)}, u32[]{:S(2)}) copy-start(bf16[1,2048,1024]{2,1,0:T(8,128)(2,1)} %param.22) | copy-start | bytes 12582916
  105.6 2.0 copy-start.1
  129.9 0.9 copy-start.3
  129.9 1.0 copy-start.4
  129.9 3.2 %copy-start.2 = (bf16[512,256]{1,0:T(8,128)(2,1)S(1)}, bf16[512,256]{1,0:T(8,128)(2,1)}, u32[]{:S(2)}) copy-start(bf16[512,256]{1,0:T(8,128)(2,1)} %param.12) | copy-start | bytes 786436
  130.0 5.1 %copy-start.7 = (f32[4]{0:T(128)S(1)}, f32[4]{0:T(128)}, u32[]{:S(2)}) copy-start(f32[4]{0:T(128)} %param.15) | copy-start | bytes 52
  130.0 79.7 %all-gather.2.cloned.1.call-start = ((), (), s32[]{:S(2)}) async-start(), calls=%async_computation.4 | async-start | bytes 1310720 | tf_op jit(solution)/shard_map/all_gather | solution.py:108
  131.7 2.8 %collective-permute-start = (bf16[128,128]{0,1:T(8,128)(2,1)S(1)}, bf16[128,128]{0,1:T(8,128)(2,1)S(1)}, u32[]{:S(2)}, u32[]{:S(2)}) collective-permute-start(bf16[128,128]{0,1:T(8,128)(2,1)S(1)} %pad_maximum_fusion.3), channel_id=1, source_target_pairs={{0,4},{4,8},{8,12},{12,16},{16,20},{20,24},{24,28},{1,5},{5,9},{9,... | collective-permute-start | bytes 98312 | tf_op jit(solution)/shard_map/ppermute | solution.py:17
  135.5 50.6 %copy-start.6 = (f32[256,2]{0,1:T(2,128)S(1)}, f32[256,2]{0,1:T(2,128)}, u32[]{:S(2)}) copy-start(f32[256,2]{0,1:T(2,128)} %param.20) | copy-start | bytes 6148
  180.8 31.7 %all-to-all-start.2 = ((bf16[512,8,128]{0,2,1:T(8,128)(2,1)}), bf16[512,8,128]{0,2,1:T(8,128)(2,1)S(1)}, u32[]{:S(2)}, u32[]{:S(2)}) async-start(bf16[512,8,128]{0,2,1:T(8,128)(2,1)} %bitcast.134), calls=%async_computation.3 | async-start | bytes 2097152 | tf_op jit(solution)/shard_map/all_to_all | solution.py:162
Sparse Core Ops, SparseCore 0:
  130.1 50.6 reduce-scatter.1
  183.2 26.4 all-gather.1
